TPU v7x, 32 devices: a whole 2x2x4 slice. The times are simulated.
32 devices in a mesh: ep: 8 (over z, core), tp: 4 (over y, x).
Axes of the slice: x: 2, y: 2, z: 4, core: 2. Of those that a mesh axis runs over, the one named last changes fastest.
Arguments:
- mixer_input: bfloat16 [2048, 2048], P('ep'), may hold values from -6 to 6
- mixer_gain: float32 [2048], replicated, may hold values from 0.1 to 1.9
- query_weight: bfloat16 [2048, 2048], P(None, 'tp'), may hold values from -0.13258252 to 0.13258252
- key_weight: bfloat16 [2048, 1024], P(None, 'tp'), may hold values from -2.78423295 to 2.78423295
- value_weight: bfloat16 [2048, 1024], P(None, 'tp'), may hold values from -0.125 to 0.125
- output_weight: bfloat16 [2048, 2048], P(None, 'tp'), may hold values from -1 to 1
- sink_logit: float32 [32], P('tp'), may hold values from 2 to 7
- expert_input: bfloat16 [1024, 2048], P('ep'), may hold values from -6 to 6
- expert_gain: float32 [2048], replicated, may hold values from 0.1 to 1.9
- routes: int32 [1024, 4], P('ep'), may hold values from 0 to 7, all different within a row; in each aligned block of 128 rows (0 to 127, 128 to 255, ...) at most 128 rows name the same one
- route_logits: float32 [1024, 4], P('ep'), may hold values from -6 to 6
- gate_weight: bfloat16 [8, 2048, 2048], P('ep', None, 'tp'), may hold values from -0.375 to 0.375
- up_weight: bfloat16 [8, 2048, 2048], P('ep', None, 'tp'), may hold values from -0.375 to 0.375
- down_weight: bfloat16 [8, 2048, 2048], P('ep', None, 'tp'), may hold values from -0.03125 to 0.03125
Outputs:
- mixer_output: bfloat16 [2048, 2048], P('ep', 'tp')
- expert_output: bfloat16 [1024, 2048], P('ep', 'tp')
Inputs may be any that keep to these rules, and one draw needn't show every extreme that they name: `routes`: each token names 4 different experts. Among the 128 tokens of one index of ep (aligned blocks) no expert is named more than 128 times, and in some blocks one expert is named exactly 128 times.
All inputs are finite; a program needn't handle non-finite values.
Results may differ from a plain program's by a relative error of at most 0.0055.
The roundings to bfloat16 on the way count: a program that leaves them out, or rounds other values in their place, can miss the bound.
Values may be sent and summed in bfloat16 or wider, within the bound.
A program may use at most 64 MiB of HBM per device.

v0:
```python
import jax
import jax.numpy as jnp
from jax import lax
from jax.sharding import PartitionSpec as P

HEAD_DIM = 64
TOP_K = 4
WINDOW = 128
GRID_W = 64
EPSILON = 1e-06
LIMIT = 7.0
SLOPE = 1.702
BASE = 10000.0


def extended(shard, sides, width):
    for axis, dim in sides:
        devices, length = (lax.axis_size(axis), shard.shape[dim])
        up = [(i, (i + 1) % devices) for i in range(devices - 1)]
        down = [(j, i) for i, j in up]
        last = lax.slice_in_dim(shard, length - width, length, axis=dim)
        first = lax.slice_in_dim(shard, 0, width, axis=dim)
        before = lax.ppermute(last, axis, up)
        after = lax.ppermute(first, axis, down)
        shard = jnp.concatenate([before, shard, after], axis=dim)
    return shard


def normalize(rows, gain):
    values = rows.astype(jnp.float32)
    scaled = values * lax.rsqrt(jnp.mean(values * values, axis=-1, keepdims=True) + EPSILON)
    return (scaled * gain).astype(jnp.bfloat16)


def turn(values, cosine, sine):
    first, second = jnp.split(values, 2, axis=-1)
    cosine = cosine[:, None, :]
    sine = sine[:, None, :]
    return jnp.concatenate(
        [first * cosine - second * sine, second * cosine + first * sine], axis=-1
    )


def axial_rope(values, places):
    quarter = values.shape[-1] // 4
    frequency = BASE ** (-jnp.arange(quarter, dtype=jnp.float32) / quarter)
    row_angle = (places // GRID_W).astype(jnp.float32)[:, None] * frequency[None, :]
    column_angle = (places % GRID_W).astype(jnp.float32)[:, None] * frequency[None, :]
    row_part, column_part = jnp.split(values, 2, axis=-1)
    return jnp.concatenate(
        [
            turn(row_part, jnp.cos(row_angle), jnp.sin(row_angle)),
            turn(column_part, jnp.cos(column_angle), jnp.sin(column_angle)),
        ],
        axis=-1,
    )


def activate(gate, up):
    capped = jnp.minimum(gate, LIMIT)
    bounded = jnp.clip(up, -LIMIT, LIMIT)
    return (capped * jax.nn.sigmoid(SLOPE * capped) * (bounded + 1.0)).astype(jnp.bfloat16)


def add_product(piece, weight):
    return jnp.dot(piece, weight, preferred_element_type=jnp.float32)


def shards(
    mixer_input,
    mixer_gain,
    query_weight,
    key_weight,
    value_weight,
    output_weight,
    sink_logit,
    expert_input,
    expert_gain,
    routes,
    route_logits,
    gate_weight,
    up_weight,
    down_weight,
):
    tokens = mixer_input.shape[0]
    query_heads = query_weight.shape[1] // HEAD_DIM
    key_heads = key_weight.shape[1] // HEAD_DIM
    group = query_heads // key_heads
    blocks = tokens // WINDOW
    offset = lax.axis_index("ep") * tokens
    length = lax.axis_size("ep") * tokens
    places = offset + jnp.arange(tokens, dtype=jnp.int32)
    normed = normalize(mixer_input, mixer_gain)
    query = jnp.dot(normed, query_weight, preferred_element_type=jnp.float32).reshape(
        tokens, query_heads, HEAD_DIM
    )
    query = (
        axial_rope(query, places)
        .astype(jnp.bfloat16)
        .reshape(blocks, WINDOW, key_heads, group, HEAD_DIM)
    )
    keys = jnp.dot(normed, key_weight, preferred_element_type=jnp.float32).reshape(
        tokens, key_heads, HEAD_DIM
    )
    keys = axial_rope(keys, places).astype(jnp.bfloat16).reshape(tokens, key_heads * HEAD_DIM)
    values = jnp.dot(normed, value_weight, preferred_element_type=jnp.float32).astype(jnp.bfloat16)
    stacked = jnp.concatenate([keys, values], axis=1)
    widened = extended(stacked, (("ep", 0),), WINDOW)
    framed = widened.reshape(blocks + 2, WINDOW, 2, key_heads, HEAD_DIM)
    nearby = jnp.concatenate([framed[:-2], framed[1:-1], framed[2:]], axis=1)
    scores = jnp.einsum(
        "nqgrd,nkgd->ngrqk", query, nearby[:, :, 0], preferred_element_type=jnp.float32
    ) * HEAD_DIM ** (-0.5)
    query_place = places.reshape(blocks, WINDOW)
    key_place = (
        offset
        + (jnp.arange(blocks, dtype=jnp.int32)[:, None] - 1) * WINDOW
        + jnp.arange(3 * WINDOW, dtype=jnp.int32)[None, :]
    )
    allowed = (
        (jnp.abs(query_place[:, :, None] - key_place[:, None, :]) <= WINDOW)
        & (key_place[:, None, :] >= 0)
        & (key_place[:, None, :] < length)
    )
    scores = jnp.where(allowed[:, None, None], scores, -1e30)
    sinks = sink_logit.reshape(key_heads, group)[None, :, :, None]
    top = jnp.maximum(jnp.max(scores, axis=-1), sinks)
    weights = jnp.exp(scores - top[..., None])
    denominator = jnp.sum(weights, axis=-1) + jnp.exp(sinks - top)
    shares = (weights / denominator[..., None]).astype(jnp.bfloat16)
    mixed = jnp.einsum(
        "ngrqk,nkgd->nqgrd", shares, nearby[:, :, 1], preferred_element_type=jnp.float32
    )
    mixed = mixed.astype(jnp.bfloat16).reshape(tokens, query_heads * HEAD_DIM)
    experts = lax.axis_size("ep")
    rows_here = expert_input.shape[0]
    capacity = 2 * rows_here * TOP_K // experts
    expert_normed = normalize(expert_input, expert_gain)
    chances = jax.nn.softmax(route_logits, axis=-1)
    chosen = routes.reshape(-1)
    marks = (chosen[:, None] == jnp.arange(experts, dtype=jnp.int32)[None, :]).astype(jnp.int32)
    earlier = jnp.sum((jnp.cumsum(marks, axis=0) - marks) * marks, axis=1)
    target = chosen * capacity + earlier
    source = (
        jnp.full((experts * capacity,), rows_here, jnp.int32)
        .at[target]
        .set(jnp.arange(chosen.shape[0], dtype=jnp.int32) // TOP_K)
    )
    padded = jnp.concatenate(
        [expert_normed, jnp.zeros((1, expert_normed.shape[1]), jnp.bfloat16)], axis=0
    )
    down_local = down_weight[0]
    gate_local = gate_weight[0]
    up_local = up_weight[0]
    width = padded.shape[1] // lax.axis_size("tp")
    own = lax.dynamic_slice_in_dim(padded, lax.axis_index("tp") * width, width, 1)
    outgoing = own[source].reshape(experts, capacity, width)
    received = lax.all_to_all(outgoing, "ep", split_axis=0, concat_axis=0, tiled=True)
    flat = received.reshape(experts * capacity, width)
    head_piece = lax.all_gather(mixed, "tp", axis=1, tiled=True)
    feature_piece = lax.all_gather(flat, "tp", axis=1, tiled=True)
    mixer_total = add_product(head_piece, output_weight)
    gate = add_product(feature_piece, gate_local)
    up = add_product(feature_piece, up_local)
    hidden = activate(gate, up)
    result = add_product(lax.all_gather(hidden, "tp", axis=1, tiled=True), down_local)
    result = result.astype(jnp.bfloat16).reshape(experts, capacity, down_local.shape[1])
    returned = lax.all_to_all(result, "ep", split_axis=0, concat_axis=0, tiled=True)
    mixer_output = mixer_total.astype(jnp.bfloat16)
    results = returned.reshape(experts * capacity, returned.shape[2])
    picked = results[target].astype(jnp.float32).reshape(rows_here, TOP_K, returned.shape[2])
    expert_output = jnp.sum(picked * chances[:, :, None], axis=1).astype(jnp.bfloat16)
    return (mixer_output, expert_output)


def solution(mesh):
    return jax.shard_map(
        shards,
        mesh=mesh,
        in_specs=(
            P("ep", None),
            P(),
            P(None, "tp"),
            P(None, "tp"),
            P(None, "tp"),
            P(None, "tp"),
            P("tp"),
            P("ep", None),
            P(),
            P("ep", None),
            P("ep", None),
            P("ep", None, "tp"),
            P("ep", None, "tp"),
            P("ep", None, "tp"),
        ),
        out_specs=(P("ep", "tp"), P("ep", "tp")),
        check_vma=False,
    )
```

profile of v0, /device:TPU:0, one launch (start us, length us, event | category | flops | bytes accessed | tf_op | source)
XLA Modules:
  0.0 214.6 jit_solution(16968832232059653629)
XLA Ops:
  9.1 1.2 fusion.19
  10.3 1.1 reduce-window.6
  12.0 2.4 %scatter_custom_fusion = s32[1024]{0:T(1024)S(1)} fusion(s32[512]{0:T(512)S(1)} %bitcast.98, s32[512]{0:T(512)S(1)} %add_select_fusion, s32[]{:T(128)} %constant.101.clone.1), kind=kCustom, calls=%fused_computation.95 | custom fusion | bytes 4100 | tf_op jit(solution)/shard_map/scatter | solution.py:147
  14.5 1.2 fusion.21
  15.8 4.0 %gather_fusion = bf16[1024,512]{1,0:T(8,128)(2,1)S(1)} fusion(bf16[129,512]{1,0:T(8,128)(2,1)S(1)} %pad_dynamic-slice_fusion, s32[1024]{0:T(1024)S(1)} %fusion.37), kind=kCustom, calls=%fused_computation | custom fusion | bytes 2101248 | tf_op jit(solution)/shard_map/gather | solution.py:157
  19.7 32.8 %all_to_all.10 = bf16[8,128,512]{2,1,0:T(8,128)(2,1)} all-to-all(bf16[8,128,512]{2,1,0:T(8,128)(2,1)S(1)} %bitcast.89), channel_id=1, replica_groups=mesh['ep'=8,'tp'=4] {'ep'}, dimensions={0} | all-to-all | bytes 2097152 | tf_op jit(solution)/shard_map/all_to_all | solution.py:158
  52.6 51.5 %all-gather.6.cloned.1.call-done = bf16[1024,2048]{1,0:T(8,128)(2,1)} async-done(((bf16[1024,512]{1,0:T(8,128)(2,1)}), bf16[1024,2048]{1,0:T(8,128)(2,1)}) %all-gather.6.cloned.1.call-update) | async-done | bytes 4194320 | tf_op jit(solution)/shard_map/all_gather | solution.py:161
  104.1 4.7 %fusion.7 = f32[1024,512]{1,0:T(8,128)S(1)} fusion(bf16[1024,2048]{1,0:T(8,128)(2,1)} %all-gather.6.cloned.1.call-done, bf16[1,2048,512]{2,1,0:T(8,128)(2,1)S(1)} %copy-done), kind=kOutput, calls=%fused_computation.15 | convolution fusion | flops 2147483648 | bytes 8388608 | tf_op jit(solution)/shard_map/dot_general | solution.py:66
  108.8 3.8 %multiply_convert_fusion = bf16[1024,512]{1,0:T(8,128)(2,1)} fusion(f32[1024,512]{1,0:T(8,128)S(1)} %fusion.7, bf16[1024,2048]{1,0:T(8,128)(2,1)S(1)} %copy-done.4, bf16[1,2048,512]{2,1,0:T(8,128)(2,1)S(1)} %copy-done.5), kind=kOutput, calls=%fused_computation.19 | convolution fusion | flops 2152726528 | bytes 9437184 | tf_op jit(solution)/shard_map/dot_general | solution.py:66
  113.4 1.9 fusion.56
  116.8 2.2 %collective-permute-start = (bf16[128,512]{0,1:T(8,128)(2,1)}, bf16[128,512]{0,1:T(8,128)(2,1)}, u32[]{:S(2)}, u32[]{:S(2)}) collective-permute-start(bf16[128,512]{0,1:T(8,128)(2,1)} %get-tuple-element.16), channel_id=1, source_target_pairs={{0,4},{4,8},{8,12},{12,16},{16,20},{20,24},{24,28},{1,5},{5,9},{9,... | collective-permute-start | bytes 393224 | tf_op jit(solution)/shard_map/ppermute | solution.py:23
  119.0 1.6 collective-permute-start.1
  120.6 1.1 fusion.53
  125.1 1.0 pad_maximum_fusion.1
  126.6 1.6 fusion.1
  131.1 34.2 %all-gather.8.cloned.1.call-done = bf16[1024,2048]{1,0:T(8,128)(2,1)} async-done(((bf16[1024,512]{1,0:T(8,128)(2,1)}), bf16[1024,2048]{1,0:T(8,128)(2,1)}) %all-gather.8.cloned.1.call-update) | async-done | bytes 4194320 | tf_op jit(solution)/shard_map/all_gather | solution.py:166
  165.3 6.2 %fusion.14 = bf16[1024,512]{1,0:T(8,128)(2,1)} fusion(bf16[1024,2048]{1,0:T(8,128)(2,1)} %all-gather.8.cloned.1.call-done, bf16[1,2048,512]{2,1,0:T(8,128)(2,1)} %param.27), kind=kOutput, calls=%fused_computation.21 | convolution fusion | flops 2148007936 | bytes 7340032 | tf_op jit(solution)/shard_map/dot_general | solution.py:66
  171.5 4.7 %all-to-all-start.1 = ((bf16[8,128,512]{2,1,0:T(8,128)(2,1)}), bf16[8,128,512]{2,1,0:T(8,128)(2,1)S(1)}, u32[]{:S(2)}, u32[]{:S(2)}) async-start(bf16[8,128,512]{2,1,0:T(8,128)(2,1)} %bitcast.93), calls=%async_computation.1 | async-start | bytes 2097152 | tf_op jit(solution)/shard_map/all_to_all | solution.py:168
  176.4 17.9 %all-gather.4.cloned.1.call-done = bf16[256,2048]{0,1:T(8,128)(2,1)} async-done(((bf16[256,512]{0,1:T(8,128)(2,1)}), bf16[256,2048]{0,1:T(8,128)(2,1)}) %all-gather.4.cloned.1.call-update) | async-done | bytes 1048592 | tf_op jit(solution)/shard_map/all_gather | solution.py:160
  194.2 3.3 %convolution_convert_fusion = bf16[256,512]{1,0:T(8,128)(2,1)} fusion(bf16[256,2048]{0,1:T(8,128)(2,1)} %all-gather.4.cloned.1.call-done, bf16[2048,512]{1,0:T(8,128)(2,1)} %param.19), kind=kOutput, calls=%fused_computation.24 | convolution fusion | flops 537001984 | bytes 3407872 | tf_op jit(solution)/shard_map/dot_general | solution.py:66
  197.6 5.2 %all-to-all-done.1 = bf16[8,128,512]{2,1,0:T(8,128)(2,1)S(1)} async-done(((bf16[8,128,512]{2,1,0:T(8,128)(2,1)}), bf16[8,128,512]{2,1,0:T(8,128)(2,1)S(1)}, u32[]{:S(2)}, u32[]{:S(2)}) %all-to-all-start.1) | async-done | bytes 1048608 | tf_op jit(solution)/shard_map/all_to_all | solution.py:168
  202.8 2.6 %gather_fusion.1 = bf16[512,512]{1,0:T(8,128)(2,1)} fusion(bf16[1024,512]{1,0:T(8,128)(2,1)S(1)} %bitcast.88, s32[1024]{0:T(1024)S(1)} %pad_clamp_fusion), kind=kCustom, calls=%fused_computation.1 | custom fusion | bytes 1050624 | tf_op jit(solution)/shard_map/gather | solution.py:171
  205.4 1.4 reshape.338
  206.7 1.4 multiply_reduce_fusion
  (83 shorter events, 11.5 us)
Async XLA Ops:
  7.2 97.0 %copy-start = (bf16[1,2048,512]{2,1,0:T(8,128)(2,1)S(1)}, bf16[1,2048,512]{2,1,0:T(8,128)(2,1)}, u32[]{:S(2)}) copy-start(bf16[1,2048,512]{2,1,0:T(8,128)(2,1)} %param.26) | copy-start | bytes 6291460
  7.2 96.9 %all-gather.6.cloned.1.call-start = ((), (), s32[]{:S(2)}) async-start(), calls=%async_computation.3 | async-start | bytes 5242880 | tf_op jit(solution)/shard_map/all_gather | solution.py:161
  52.6 112.7 %all-gather.8.cloned.1.call-start = ((), (), s32[]{:S(2)}) async-start(), calls=%async_computation.4 | async-start | bytes 5242880 | tf_op jit(solution)/shard_map/all_gather | solution.py:166
  104.1 4.7 %copy-start.4 = (bf16[1024,2048]{1,0:T(8,128)(2,1)S(1)}, bf16[1024,2048]{1,0:T(8,128)(2,1)}, u32[]{:S(2)}) copy-start(bf16[1024,2048]{1,0:T(8,128)(2,1)} %all-gather.6.cloned.1.call-done) | copy-start | bytes 12582916
  104.1 4.7 %copy-start.5 = (bf16[1,2048,512]{2,1,0:T(8,128)(2,1)S(1)}, bf16[1,2048,512]{2,1,0:T(8,128)(2,1)}, u32[]{:S(2)}) copy-start(bf16[1,2048,512]{2,1,0:T(8,128)(2,1)} %param.25) | copy-start | bytes 6291460
  108.8 4.0 %copy-start.1 = (bf16[256,2048]{1,0:T(8,128)(2,1)S(1)}, bf16[256,2048]{1,0:T(8,128)(2,1)}, u32[]{:S(2)}) copy-start(bf16[256,2048]{1,0:T(8,128)(2,1)} %param.14) | copy-start | bytes 3145732
  112.7 0.7 copy-start.8
  112.7 81.5 %all-gather.4.cloned.1.call-start = ((), (), s32[]{:S(2)}) async-start(), calls=%async_computation.2 | async-start | bytes 1310720 | tf_op jit(solution)/shard_map/all_gather | solution.py:160
  113.1 2.3 %copy-start.7 = (bf16[2048,256]{1,0:T(8,128)(2,1)S(1)}, bf16[2048,256]{1,0:T(8,128)(2,1)}, u32[]{:S(2)}) copy-start(bf16[2048,256]{1,0:T(8,128)(2,1)} %param.18) | copy-start | bytes 3145732
  115.3 5.3 %copy-start.6 = (bf16[2048,512]{1,0:T(8,128)(2,1)S(1)}, bf16[2048,512]{1,0:T(8,128)(2,1)}, u32[]{:S(2)}) copy-start(bf16[2048,512]{1,0:T(8,128)(2,1)} %param.16) | copy-start | bytes 6291460
  116.8 8.3 %collective-permute-start = (bf16[128,512]{0,1:T(8,128)(2,1)}, bf16[128,512]{0,1:T(8,128)(2,1)}, u32[]{:S(2)}, u32[]{:S(2)}) collective-permute-start(bf16[128,512]{0,1:T(8,128)(2,1)} %get-tuple-element.16), channel_id=1, source_target_pairs={{0,4},{4,8},{8,12},{12,16},{16,20},{20,24},{24,28},{1,5},{5,9},{9,... | collective-permute-start | bytes 393224 | tf_op jit(solution)/shard_map/ppermute | solution.py:23
  119.0 5.4 %copy-start.3 = (f32[8]{0:T(128)S(1)}, f32[8]{0:T(128)}, u32[]{:S(2)}) copy-start(f32[8]{0:T(128)} %param.20) | copy-start | bytes 100
  119.0 6.1 %collective-permute-start.1 = (bf16[128,512]{0,1:T(8,128)(2,1)}, bf16[128,512]{0,1:T(8,128)(2,1)}, u32[]{:S(2)}, u32[]{:S(2)}) collective-permute-start(bf16[128,512]{0,1:T(8,128)(2,1)} %get-tuple-element.15), channel_id=1, source_target_pairs={{4,0},{8,4},{12,8},{16,12},{20,16},{24,20},{28,24},{5,1},{9,5},{13... | collective-permute-start | bytes 393224 | tf_op jit(solution)/shard_map/ppermute | solution.py:24
  171.5 4.7 %copy-start.2 = (f32[128,4]{0,1:T(4,128)S(1)}, f32[128,4]{0,1:T(4,128)}, u32[]{:S(2)}) copy-start(f32[128,4]{0,1:T(4,128)} %param.24) | copy-start | bytes 6148
  171.5 31.3 %all-to-all-start.1 = ((bf16[8,128,512]{2,1,0:T(8,128)(2,1)}), bf16[8,128,512]{2,1,0:T(8,128)(2,1)S(1)}, u32[]{:S(2)}, u32[]{:S(2)}) async-start(bf16[8,128,512]{2,1,0:T(8,128)(2,1)} %bitcast.93), calls=%async_computation.1 | async-start | bytes 2097152 | tf_op jit(solution)/shard_map/all_to_all | solution.py:168
Sparse Core Ops, SparseCore 0:
  52.7 51.3 all-gather.5
  112.8 52.4 all-gather.7
  167.7 26.4 all-gather.3
where the time goes:
time: 215 us
  waiting for transfers between devices  109 us (51%)
  blocking collectives  32.8 us (15%)
  matrix products  24.2 us (11%)
  local copies, waits for them, and re-layouts  16.3 us (8%)
  between operations  14.1 us (7%)
  other arithmetic  9.73 us (5%)
  starting transfers between devices  8.66 us (4%)
    all_gather x1, waiting for transfers between devices, shards(): feature_piece = lax.all_gather(flat, 'tp', axis=1, tiled=True)  51.5 us
    all_gather x1, waiting for transfers between devices, shards(): lax.all_gather(hidden, 'tp', axis=1, tiled=True)  34.2 us
    all_to_all x1, blocking collectives, shards(): lax.all_to_all(outgoing, 'ep', split_axis=0, concat_axis=0, tiled=True)  32.8 us
    dot_general x4, matrix products, add_product(): return jnp.dot(piece, weight, preferred_element_type=jnp.float32)  18 us
    all_gather x1, waiting for transfers between devices, shards(): head_piece = lax.all_gather(mixed, 'tp', axis=1, tiled=True)  17.9 us
    all_to_all x1, waiting for transfers between devices, shards(): lax.all_to_all(result, 'ep', split_axis=0, concat_axis=0, tiled=True)  5.17 us
    all_to_all x1, starting transfers between devices, shards(): lax.all_to_all(result, 'ep', split_axis=0, concat_axis=0, tiled=True)  4.74 us
  transfers between devices with their start and end apart: 6, of which 4 were waited for; matrix products, arithmetic and copies ran while one was open for 11% of the time, Pallas kernels for 0%

commit v1 on v0

--- a/solution.py
+++ b/solution.py
@@ -157,8 +157,11 @@
     outgoing = own[source].reshape(experts, capacity, width)
     received = lax.all_to_all(outgoing, "ep", split_axis=0, concat_axis=0, tiled=True)
     flat = received.reshape(experts * capacity, width)
-    head_piece = lax.all_gather(mixed, "tp", axis=1, tiled=True)
-    feature_piece = lax.all_gather(flat, "tp", axis=1, tiled=True)
+    head_piece, feature_piece = jnp.split(
+        lax.all_gather(jnp.concatenate([mixed, flat], axis=0), "tp", axis=1, tiled=True),
+        [mixed.shape[0]],
+        axis=0,
+    )
     mixer_total = add_product(head_piece, output_weight)
     gate = add_product(feature_piece, gate_local)
     up = add_product(feature_piece, up_local)

time: 215 us -> 245 us (1.14)
  waiting for transfers between devices: 109 us -> 143 us
  blocking collectives: 32.8 us -> 0 us
  local copies, waits for them, and re-layouts: 16.3 us -> 29.9 us
  starting transfers between devices: 8.66 us -> 16.4 us
  other arithmetic: 9.73 us -> 16.3 us
    all_to_all x1 -> x0, blocking collectives: 32.8 us -> none  [shards(): lax.all_to_all(outgoing, 'ep', split_axis=0, concat_axis=0, tiled=True)]
    all_gather x1, waiting for transfers between devices: 34.2 us -> 52.6 us  [shards(): lax.all_gather(hidden, 'tp', axis=1, tiled=True)]
    all_to_all x1, waiting for transfers between devices: 5.17 us -> 23 us  [shards(): lax.all_to_all(result, 'ep', split_axis=0, concat_axis=0, tiled=True)]
    all_to_all x0 -> x1, starting transfers between devices: none -> 6.49 us  [shards(): lax.all_to_all(outgoing, 'ep', split_axis=0, concat_axis=0, tiled=True)]
    slice x3, local copies, waits for them, and re-layouts: 0.2 us -> 4.26 us  [shards(): nearby = jnp.concatenate([framed[:-2], framed[1:-1], framed[2:]], axis=1)]
    unnamed x22 -> x25, local copies, waits for them, and re-layouts: 1.9 us -> 4.99 us
    reshape x0 -> x2, local copies, waits for them, and re-layouts: none -> 2.49 us  [shards(): mixed = mixed.astype(jnp.bfloat16).reshape(tokens, query_heads * HEAD_DIM)]
    all_gather x2 -> x1, waiting for transfers between devices: 69.3 us -> 67.1 us  [shards(): lax.all_gather(jnp.concatenate([mixed, flat], axis=0), 'tp', axis=1, tile...]
  transfers between devices with their start and end apart: 6 -> 6, of which waited for: 4 -> 3; matrix products, arithmetic and copies ran while one was open for 11% -> 14% of each run, Pallas kernels for 0% -> 0%
where the time goes in v1:
time: 245 us; the launch traced here: 244 us
  waiting for transfers between devices  143 us (58%)
  local copies, waits for them, and re-layouts  29.9 us (12%)
  matrix products  24.7 us (10%)
  starting transfers between devices  16.4 us (7%)
  other arithmetic  16.3 us (7%)
  between operations  14.3 us (6%)
    all_gather x1, waiting for transfers between devices, shards(): lax.all_gather(jnp.concatenate([mixed, flat], axis=0), 'tp', axis=1, tile...  67.1 us
    all_gather x1, waiting for transfers between devices, shards(): lax.all_gather(hidden, 'tp', axis=1, tiled=True)  52.6 us
    all_to_all x1, waiting for transfers between devices, shards(): lax.all_to_all(result, 'ep', split_axis=0, concat_axis=0, tiled=True)  23 us
    dot_general x4, matrix products, add_product(): return jnp.dot(piece, weight, preferred_element_type=jnp.float32)  18 us
    all_to_all x1, starting transfers between devices, shards(): lax.all_to_all(outgoing, 'ep', split_axis=0, concat_axis=0, tiled=True)  6.49 us
    gather x1, local copies, waits for them, and re-layouts, shards(): outgoing = own[source].reshape(experts, capacity, width)  5.07 us
    unnamed x25, local copies, waits for them, and re-layouts  4.99 us
  transfers between devices with their start and end apart: 6, of which 3 were waited for; matrix products, arithmetic and copies ran while one was open for 14% of the time, Pallas kernels for 0%

profile of v1, /device:TPU:0, one launch (start us, length us, event | category | flops | bytes accessed | tf_op | source)
XLA Modules:
  0.0 244.5 jit_solution(4478326148117019532)
XLA Ops:
  12.0 2.4 %scatter_custom_fusion = s32[1024]{0:T(1024)S(1)} fusion(s32[512]{0:T(512)S(1)} %bitcast.85, s32[512]{0:T(512)S(1)} %add_select_fusion, s32[]{:T(128)} %constant.101.clone.1), kind=kCustom, calls=%fused_computation.98 | custom fusion | bytes 4100 | tf_op jit(solution)/shard_map/scatter | solution.py:147
  15.8 5.1 %gather_fusion = bf16[1024,512]{1,0:T(8,128)(2,1)} fusion(bf16[129,512]{1,0:T(8,128)(2,1)S(1)} %pad_dynamic-slice_fusion, s32[1024]{0:T(1024)S(1)} %fusion.42), kind=kCustom, calls=%fused_computation | custom fusion | bytes 2101248 | tf_op jit(solution)/shard_map/gather | solution.py:157
  20.8 6.5 %all-to-all-start = ((bf16[8,128,512]{2,1,0:T(8,128)(2,1)}), bf16[8,128,512]{2,1,0:T(8,128)(2,1)S(1)}, u32[]{:S(2)}, u32[]{:S(2)}) async-start(bf16[8,128,512]{2,1,0:T(8,128)(2,1)} %bitcast.15), calls=%async_computation | async-start | bytes 2097152 | tf_op jit(solution)/shard_map/all_to_all | solution.py:158
  27.4 1.5 fusion.6
  29.0 2.3 fusion.61
  34.7 3.7 %collective-permute-start = (bf16[128,512]{0,1:T(8,128)(2,1)}, bf16[128,512]{0,1:T(8,128)(2,1)}, u32[]{:S(2)}, u32[]{:S(2)}) collective-permute-start(bf16[128,512]{0,1:T(8,128)(2,1)} %get-tuple-element.16), channel_id=1, source_target_pairs={{0,4},{4,8},{8,12},{12,16},{16,20},{20,24},{24,28},{1,5},{5,9},{9,... | collective-permute-start | bytes 393224 | tf_op jit(solution)/shard_map/ppermute | solution.py:23
  45.6 1.8 fusion.29
  47.4 2.0 pad_maximum_fusion.2
  49.4 1.8 slice.46
  51.1 1.7 copy_dynamic-update-slice_fusion.2
  52.9 1.7 slice.47
  55.4 1.8 copy_dynamic-update-slice_fusion.1
  57.1 1.7 copy_dynamic-update-slice_fusion
  58.8 1.7 fusion.5
  63.8 1.4 reshape.366
  66.6 67.1 %all-gather.3.cloned.1.call-done = bf16[1280,2048]{1,0:T(8,128)(2,1)} async-done(((bf16[1280,512]{1,0:T(8,128)(2,1)}), bf16[1280,2048]{1,0:T(8,128)(2,1)}) %all-gather.3.cloned.1.call-update) | async-done | bytes 5242896 | tf_op jit(solution)/shard_map/all_gather | solution.py:161
  133.7 4.7 %fusion = f32[1024,512]{1,0:T(8,128)S(1)} fusion(bf16[1280,2048]{1,0:T(8,128)(2,1)} %all-gather.3.cloned.1.call-done, bf16[1,2048,512]{2,1,0:T(8,128)(2,1)S(1)} %copy-done), kind=kOutput, calls=%fused_computation.3 | convolution fusion | flops 2147483648 | bytes 8388608 | tf_op jit(solution)/shard_map/dot_general | solution.py:66
  138.4 3.8 %multiply_convert_fusion = bf16[1024,512]{1,0:T(8,128)(2,1)} fusion(f32[1024,512]{1,0:T(8,128)S(1)} %fusion, bf16[1,2048,512]{2,1,0:T(8,128)(2,1)S(1)} %copy-done.8, bf16[1280,2048]{1,0:T(8,128)(2,1)S(1)} %copy-done.6), kind=kOutput, calls=%fused_computation.21 | convolution fusion | flops 2152726528 | bytes 9437184 | tf_op jit(solution)/shard_map/dot_general | solution.py:66
  142.2 52.6 %all-gather.5.cloned.1.call-done = bf16[1024,2048]{1,0:T(8,128)(2,1)} async-done(((bf16[1024,512]{1,0:T(8,128)(2,1)}), bf16[1024,2048]{1,0:T(8,128)(2,1)}) %all-gather.5.cloned.1.call-update) | async-done | bytes 4194320 | tf_op jit(solution)/shard_map/all_gather | solution.py:169
  194.8 6.2 %fusion.18 = bf16[1024,512]{1,0:T(8,128)(2,1)} fusion(bf16[1024,2048]{1,0:T(8,128)(2,1)} %all-gather.5.cloned.1.call-done, bf16[1,2048,512]{2,1,0:T(8,128)(2,1)} %param.27), kind=kOutput, calls=%fused_computation.23 | convolution fusion | flops 2148007936 | bytes 7340032 | tf_op jit(solution)/shard_map/dot_general | solution.py:66
  201.0 4.7 %all-to-all-start.1 = ((bf16[8,128,512]{2,1,0:T(8,128)(2,1)}), bf16[8,128,512]{2,1,0:T(8,128)(2,1)S(1)}, u32[]{:S(2)}, u32[]{:S(2)}) async-start(bf16[8,128,512]{2,1,0:T(8,128)(2,1)} %bitcast.82), calls=%async_computation.1 | async-start | bytes 2097152 | tf_op jit(solution)/shard_map/all_to_all | solution.py:171
  205.9 3.3 %convolution_convert_fusion = bf16[256,512]{1,0:T(8,128)(2,1)} fusion(bf16[2048,512]{1,0:T(8,128)(2,1)} %param.19, bf16[1280,2048]{1,0:T(8,128)(2,1)} %all-gather.3.cloned.1.call-done), kind=kOutput, calls=%fused_computation.27 | convolution fusion | flops 537001984 | bytes 3407872 | tf_op jit(solution)/shard_map/dot_general | solution.py:66
  209.2 23.0 %all-to-all-done.1 = bf16[8,128,512]{2,1,0:T(8,128)(2,1)S(1)} async-done(((bf16[8,128,512]{2,1,0:T(8,128)(2,1)}), bf16[8,128,512]{2,1,0:T(8,128)(2,1)S(1)}, u32[]{:S(2)}, u32[]{:S(2)}) %all-to-all-start.1) | async-done | bytes 1048608 | tf_op jit(solution)/shard_map/all_to_all | solution.py:171
  232.3 2.6 %gather_fusion.1 = bf16[512,512]{1,0:T(8,128)(2,1)} fusion(bf16[1024,512]{1,0:T(8,128)(2,1)S(1)} %bitcast.78, s32[1024]{0:T(1024)S(1)} %pad_clamp_fusion), kind=kCustom, calls=%fused_computation.1 | custom fusion | bytes 1050624 | tf_op jit(solution)/shard_map/gather | solution.py:174
  (86 shorter events, 25.1 us)
Async XLA Ops:
  7.2 126.5 %copy-start = (bf16[1,2048,512]{2,1,0:T(8,128)(2,1)S(1)}, bf16[1,2048,512]{2,1,0:T(8,128)(2,1)}, u32[]{:S(2)}) copy-start(bf16[1,2048,512]{2,1,0:T(8,128)(2,1)} %param.26) | copy-start | bytes 6291460
  20.8 8.1 %copy-start.10 = (f32[2048]{0:T(1024)S(1)}, f32[2048]{0:T(1024)}, u32[]{:S(2)}) copy-start(f32[2048]{0:T(1024)} %param.15) | copy-start | bytes 24580
  20.8 44.3 %all-to-all-start = ((bf16[8,128,512]{2,1,0:T(8,128)(2,1)}), bf16[8,128,512]{2,1,0:T(8,128)(2,1)S(1)}, u32[]{:S(2)}, u32[]{:S(2)}) async-start(bf16[8,128,512]{2,1,0:T(8,128)(2,1)} %bitcast.15), calls=%async_computation | async-start | bytes 2097152 | tf_op jit(solution)/shard_map/all_to_all | solution.py:158
  27.3 106.4 %all-gather.3.cloned.1.call-start = ((), (), s32[]{:S(2)}) async-start(), calls=%async_computation.2 | async-start | bytes 6553600 | tf_op jit(solution)/shard_map/all_gather | solution.py:161
  28.9 2.4 copy-start.1
  28.9 2.4 copy-start.9
  31.3 8.3 %copy-start.7 = (bf16[2048,512]{1,0:T(8,128)(2,1)S(1)}, bf16[2048,512]{1,0:T(8,128)(2,1)}, u32[]{:S(2)}) copy-start(bf16[2048,512]{1,0:T(8,128)(2,1)} %param.16) | copy-start | bytes 6291460
  32.0 0.7 copy-start.2
  33.4 14.0 %collective-permute-start.1 = (bf16[128,512]{0,1:T(8,128)(2,1)}, bf16[128,512]{0,1:T(8,128)(2,1)}, u32[]{:S(2)}, u32[]{:S(2)}) collective-permute-start(bf16[128,512]{0,1:T(8,128)(2,1)} %get-tuple-element.15), channel_id=1, source_target_pairs={{4,0},{8,4},{12,8},{16,12},{20,16},{24,20},{28,24},{5,1},{9,5},{13... | collective-permute-start | bytes 393224 | tf_op jit(solution)/shard_map/ppermute | solution.py:24
  34.7 12.7 %collective-permute-start = (bf16[128,512]{0,1:T(8,128)(2,1)}, bf16[128,512]{0,1:T(8,128)(2,1)}, u32[]{:S(2)}, u32[]{:S(2)}) collective-permute-start(bf16[128,512]{0,1:T(8,128)(2,1)} %get-tuple-element.16), channel_id=1, source_target_pairs={{0,4},{4,8},{8,12},{12,16},{16,20},{20,24},{24,28},{1,5},{5,9},{9,... | collective-permute-start | bytes 393224 | tf_op jit(solution)/shard_map/ppermute | solution.py:23
  49.4 9.5 %copy-start.3 = (pred[2,128,384]{1,2,0:T(8,128)(4,1)S(1)}, pred[2,128,384]{1,2,0:T(8,128)(4,1)}, u32[]{:S(2)}) copy-start(pred[2,128,384]{1,2,0:T(8,128)(4,1)} %fusion.29) | copy-start | bytes 294916
  60.6 1.1 copy-start.4
  66.4 128.5 %all-gather.5.cloned.1.call-start = ((), (), s32[]{:S(2)}) async-start(), calls=%async_computation.3 | async-start | bytes 5242880 | tf_op jit(solution)/shard_map/all_gather | solution.py:169
  133.7 4.7 %copy-start.6 = (bf16[1280,2048]{1,0:T(8,128)(2,1)S(1)}, bf16[1280,2048]{1,0:T(8,128)(2,1)}, u32[]{:S(2)}) copy-start(bf16[1280,2048]{1,0:T(8,128)(2,1)} %all-gather.3.cloned.1.call-done) | copy-start | bytes 15728644
  133.7 4.7 %copy-start.8 = (bf16[1,2048,512]{2,1,0:T(8,128)(2,1)S(1)}, bf16[1,2048,512]{2,1,0:T(8,128)(2,1)}, u32[]{:S(2)}) copy-start(bf16[1,2048,512]{2,1,0:T(8,128)(2,1)} %param.25) | copy-start | bytes 6291460
  201.0 4.7 %copy-start.5 = (f32[128,4]{0,1:T(4,128)S(1)}, f32[128,4]{0,1:T(4,128)}, u32[]{:S(2)}) copy-start(f32[128,4]{0,1:T(4,128)} %param.24) | copy-start | bytes 6148
  201.0 31.3 %all-to-all-start.1 = ((bf16[8,128,512]{2,1,0:T(8,128)(2,1)}), bf16[8,128,512]{2,1,0:T(8,128)(2,1)S(1)}, u32[]{:S(2)}, u32[]{:S(2)}) async-start(bf16[8,128,512]{2,1,0:T(8,128)(2,1)} %bitcast.82), calls=%async_computation.1 | async-start | bytes 2097152 | tf_op jit(solution)/shard_map/all_to_all | solution.py:171
Sparse Core Ops, SparseCore 0:
  66.5 67.1 all-gather.2
  142.3 52.4 all-gather.4
